TPU v7x, 32 devices: a whole 2x2x4 slice. The times are simulated.
32 devices in a mesh: rep: 2 (over x), fs: 8 (over z, y), tp: 2 (over core).
Axes of the slice: x: 2, y: 2, z: 4, core: 2. Of those that a mesh axis runs over, the one named last changes fastest.
Arguments:
- inputs: bfloat16 [2, 3072, 2048], P('rep', 'fs', 'tp'), may hold values from -6 to 6
- gate_proj: bfloat16 [2048, 2816], P('fs', 'tp'), may hold values from -0.125 to 0.125
- value_proj: bfloat16 [2048, 2816], P('fs', 'tp'), may hold values from -0.125 to 0.125
- gate_taps: float32 [3, 2816], replicated, may hold values from -3 to 3
- value_taps: float32 [3, 2816], replicated, may hold values from -3 to 3
- out_grad: bfloat16 [2, 3072, 2816], P('rep', 'fs', 'tp'), may hold values from -6 to 6
Outputs:
- in_grad: bfloat16 [2, 3072, 2048], P('rep', 'fs', 'tp')
- gate_proj_grad: float32 [2048, 2816], P('fs', 'tp')
- value_proj_grad: float32 [2048, 2816], P('fs', 'tp')
- gate_taps_grad: float32 [3, 2816], replicated
- value_taps_grad: float32 [3, 2816], replicated
All inputs are finite; a program needn't handle non-finite values.
Results may differ from a plain program's by a relative error of at most 0.013.
Values may be sent and summed in bfloat16 or wider, within the bound.
A program may use at most 128 MiB of HBM per device.

v0:
```python
import jax
import jax.numpy as jnp
from jax import lax
from jax.sharding import PartitionSpec as P

HALO = 8


def shift(x, axis, step):
    count = lax.axis_size(axis)
    return lax.ppermute(x, axis, [(i, (i + step) % count) for i in range(count)])


def with_halo(rows):
    count = lax.axis_size("fs")
    nxt = lax.ppermute(rows[:HALO], "fs", [(i + 1, i) for i in range(count - 1)])
    prv = lax.ppermute(rows[rows.shape[0] - HALO :], "fs", [(i, i + 1) for i in range(count - 1)])
    return jnp.concatenate([rows, nxt, prv], axis=0)


def before(x):
    return jnp.concatenate([x[:, -1:], x[:, :-1]], axis=1)


def after(x):
    return jnp.concatenate([x[:, 1:], x[:, :1]], axis=1)


def shards(inputs, gate_proj, value_proj, gate_taps, value_taps, out_grad):
    contract_cols = (((1,), (1,)), ((), ()))
    contract_rows = (((0,), (0,)), ((), ()))
    reps, fs_count = (lax.axis_size("rep"), lax.axis_size("fs"))
    rep = lax.axis_index("rep")
    tokens, feats = inputs.shape[1:]
    hid = gate_proj.shape[1]
    width = min(hid, -(-hid // reps // 128) * 128)
    last = hid - width

    def start_of(part):
        return jnp.minimum(part * width, last)

    first = start_of(rep)
    dead = rep * width - first
    live = jnp.arange(width) >= dead

    def part_cols(x, part):
        return lax.dynamic_slice_in_dim(x, start_of(part), width, x.ndim - 1)

    w_own = jnp.concatenate(
        [
            jnp.where(live, part_cols(w, rep), jnp.zeros((), w.dtype))
            for w in (gate_proj, value_proj)
        ],
        axis=1,
    )
    w_all = lax.all_gather(w_own, "fs", axis=0, tiled=True)
    x_ext = with_halo(inputs[0])
    g_ext = with_halo(out_grad[0])
    x_blocks, g_blocks = ([x_ext], [part_cols(g_ext, rep)])
    for step in range(1, reps):
        x_blocks.append(shift(x_ext, "rep", step))
        g_blocks.append(shift(part_cols(g_ext, (rep + step) % reps), "rep", step))
    x_all = lax.all_gather(jnp.stack(x_blocks), "tp", axis=2, tiled=True)
    g_all = jnp.stack(g_blocks).astype(jnp.float32)
    ext = tokens + 2 * HALO
    pre = jnp.dot(x_all.reshape(reps * ext, -1), w_all, preferred_element_type=jnp.float32)
    pre = pre.astype(jnp.bfloat16).astype(jnp.float32).reshape(reps, ext, 2 * width)
    tap_start = lax.axis_index("tp") * hid + first
    taps = jnp.concatenate(
        [lax.dynamic_slice_in_dim(t, tap_start, width, 1) for t in (gate_taps, value_taps)], axis=1
    )
    pre_b, pre_a = (before(pre), after(pre))
    mix = taps[0] * pre_b + taps[1] * pre + taps[2] * pre_a
    gate_mix, value_mix = (mix[..., :width], mix[..., width:])
    sig = jax.nn.sigmoid(gate_mix)
    gate_cot = g_all * value_mix * (sig * (1.0 + gate_mix * (1.0 - sig)))
    value_cot = g_all * (gate_mix * sig)
    cot = jnp.concatenate([gate_cot, value_cot], axis=2)
    pre_cot = taps[0] * after(cot) + taps[1] * cot + taps[2] * before(cot)
    pre_cot = pre_cot[:, :tokens].astype(jnp.bfloat16).reshape(reps * tokens, 2 * width)
    tap_terms = jnp.stack(
        [jnp.sum(p[:, :tokens] * cot[:, :tokens], axis=(0, 1)) for p in (pre_b, pre, pre_a)]
    )
    factor = float(tokens * fs_count * reps) ** (-0.5)
    grads = lax.dot_general(
        x_all[:, :tokens].reshape(reps * tokens, -1),
        pre_cot,
        contract_rows,
        preferred_element_type=jnp.float32,
    )
    grads = (grads * factor).astype(jnp.bfloat16)
    own = lax.psum_scatter(grads, "fs", scatter_dimension=0, tiled=True)
    partial_value = lax.dot_general(
        pre_cot, w_all, contract_cols, preferred_element_type=jnp.float32
    )
    partial_value = lax.psum_scatter(
        partial_value.astype(jnp.bfloat16), "tp", scatter_dimension=1, tiled=True
    ).reshape(reps, tokens, feats)
    in_grad = partial_value[0].astype(jnp.float32)
    for step in range(1, reps):
        in_grad += shift(partial_value[step], "rep", -step).astype(jnp.float32)
    blocks = [own]
    for step in range(1, reps):
        blocks.append(shift(own, "rep", step))
    proj_grads = []
    for branch in range(2):
        cols = jnp.zeros((own.shape[0], hid), jnp.bfloat16)
        cut = [b[:, branch * width : (branch + 1) * width] for b in blocks]
        for step in range(reps):
            part = (rep - step) % reps
            place = start_of(part)
            skip = part * width - place
            old = lax.dynamic_slice_in_dim(cols, place, width, 1)
            new = jnp.where(jnp.arange(width) >= skip, cut[step], old)
            cols = lax.dynamic_update_slice_in_dim(cols, new, place, 1)
        proj_grads.append(cols.astype(jnp.float32))
    tap_sum = lax.psum(tap_terms * factor, "fs").reshape(3, 2, width)
    tap_all = lax.all_gather(lax.all_gather(tap_sum, "rep"), "tp")
    halves = []
    for half in range(tap_all.shape[0]):
        cols = [
            tap_all[half, p, :, :, max(0, p * width - last) if p * width > last else 0 :]
            for p in range(reps)
        ]
        halves.append(jnp.concatenate(cols, axis=2))
    taps_out = jnp.concatenate(halves, axis=2)
    return (
        in_grad.astype(jnp.bfloat16)[None],
        proj_grads[0],
        proj_grads[1],
        taps_out[:, 0],
        taps_out[:, 1],
    )


def solution(mesh):
    placed = (P("rep", "fs", "tp"), P("fs", "tp"), P("fs", "tp"), P(), P(), P("rep", "fs", "tp"))
    return jax.shard_map(
        shards,
        mesh=mesh,
        in_specs=placed,
        out_specs=(P("rep", "fs", "tp"), P("fs", "tp"), P("fs", "tp"), P(), P()),
        check_vma=False,
    )
```

profile of v0, /device:TPU:2, one launch (start us, length us, event | category | flops | bytes accessed | tf_op | source)
XLA Modules:
  0.0 368.1 jit_solution(3353467001362223861)
XLA Ops:
  7.2 1.5 copy.18
  8.8 3.4 collective-permute-start.4
  12.3 1.3 collective-permute-start.3
  13.6 9.8 %collective-permute-done.4 = bf16[8,1024]{0,1:T(8,128)(2,1)S(1)} collective-permute-done((bf16[8,1024]{0,1:T(8,128)(2,1)S(1)}, bf16[8,1024]{0,1:T(8,128)(2,1)S(1)}, u32[]{:S(2)}, u32[]{:S(2)}) %collective-permute-start.4) | collective-permute-done | bytes 16416 | tf_op jit(solution)/shard_map/ppermute | solution.py:17
  24.9 16.7 %collective-permute-done.5 = bf16[400,1024]{1,0:T(8,128)(2,1)} collective-permute-done((bf16[400,1024]{1,0:T(8,128)(2,1)S(1)}, bf16[400,1024]{1,0:T(8,128)(2,1)}, u32[]{:S(2)}, u32[]{:S(2)}) %collective-permute-start.5) | collective-permute-done | bytes 819232 | tf_op jit(solution)/shard_map/ppermute | solution.py:11
  41.6 1.4 copy.22
  43.1 1.6 pad_maximum_fusion.4
  44.8 1.5 dynamic-slice_select_fusion.1
  47.3 6.2 %collective-permute-start.1 = (bf16[8,1408]{1,0:T(8,128)(2,1)S(1)}, bf16[8,1408]{1,0:T(8,128)(2,1)S(1)}, u32[]{:S(2)}, u32[]{:S(2)}) collective-permute-start(bf16[8,1408]{1,0:T(8,128)(2,1)S(1)} %get-tuple-element.25), channel_id=1, source_target_pairs={{0,2},{2,4},{4,6},{6,8},{8,10},{10,12},{12,14},{1,3},{3,5},{5,7},{... | collective-permute-start | bytes 67592 | tf_op jit(solution)/shard_map/ppermute | solution.py:17
  53.5 1.5 collective-permute-start
  55.9 4.8 %collective-permute-done = bf16[8,1408]{1,0:T(8,128)(2,1)S(1)} collective-permute-done((bf16[8,1408]{1,0:T(8,128)(2,1)S(1)}, bf16[8,1408]{1,0:T(8,128)(2,1)S(1)}, u32[]{:S(2)}, u32[]{:S(2)}) %collective-permute-start) | collective-permute-done | bytes 22560 | tf_op jit(solution)/shard_map/ppermute | solution.py:16
  60.7 1.6 dynamic-slice_bitcast_fusion
  63.7 4.7 %copy.23 = bf16[2,400,2048]{2,1,0:T(8,128)(2,1)S(1)} copy(bf16[2,400,2048]{1,2,0:T(8,128)(2,1)} %all-gather.4.cloned.1.call-done) | data formatting | bytes 6553600 | tf_op jit(solution)/shard_map/all_gather | solution.py:63
  68.4 97.7 %all-gather.6.cloned.1.call-done = bf16[2048,1536]{1,0:T(8,128)(2,1)} async-done(((bf16[256,1536]{1,0:T(8,128)(2,1)}), bf16[2048,1536]{1,0:T(8,128)(2,1)}) %all-gather.6.cloned.1.call-update) | async-done | bytes 6291472 | tf_op jit(solution)/shard_map/all_gather | solution.py:56
  166.1 8.2 %convolution_convert_fusion = bf16[800,1536]{1,0:T(8,128)(2,1)S(1)} fusion(bf16[800,2048]{1,0:T(8,128)(2,1)S(1)} %bitcast.55, bf16[2048,1536]{1,0:T(8,128)(2,1)} %all-gather.6.cloned.1.call-done), kind=kOutput, calls=%fused_computation.37 | convolution fusion | flops 5034393600 | bytes 12025856 | tf_op jit(solution)/shard_map/dot_general | solution.py:66
  175.0 1.3 fusion.24
  176.3 1.7 fusion.3
  178.0 2.2 convert_multiply_fusion
  181.3 8.2 %fusion.15 = (f32[1536]{0:T(1024)S(1)}, f32[1536]{0:T(1024)S(1)}, f32[1536]{0:T(1024)S(1)}, bf16[2,384,1536]{2,1,0:T(8,128)(2,1)S(1)}) fusion(f32[2,400,1536]{2,1,0:T(8,128)S(1)} %convert.5, f32[2,400,768]{2,1,0:T(8,128)S(1)} %get-tuple-element.11, f32[2,400,768]{2,1,0:T(8,128)S(1)} %get-tuple-element.12, f32[2,399,1536]{2,1,0:T(8,128)S(1)} %get-tuple-element.18, ...), kind=kLoop, calls=%fused_computation.31 | loop fusion | flops 20049408 | bytes 31494144 | tf_op jit(solution)/shard_map/reduce_sum | solution.py:82
  189.6 9.3 %convolution_convert_fusion.1 = bf16[768,2048]{1,0:T(8,128)(2,1)} fusion(bf16[768,1536]{1,0:T(8,128)(2,1)S(1)} %bitcast.56, bf16[2048,1536]{1,0:T(8,128)(2,1)} %all-gather.6.cloned.1.call-done), kind=kOutput, calls=%fused_computation.38 | convolution fusion | flops 4833411072 | bytes 11796480 | tf_op jit(solution)/shard_map/dot_general | solution.py:93
  199.2 8.9 %fusion = bf16[2048,1536]{1,0:T(8,128)(2,1)} fusion(bf16[2,384,1536]{2,1,0:T(8,128)(2,1)S(1)} %get-tuple-element.13, bf16[2,400,2048]{1,2,0:T(8,128)(2,1)} %all-gather.4.cloned.1.call-done), kind=kOutput, calls=%fused_computation.1 | convolution fusion | flops 4838129664 | bytes 11796480 | tf_op jit(solution)/shard_map/dot_general | solution.py:85
  208.3 35.4 %psum.7 = f32[1,3,2,768]{3,2,1,0:T(2,128)S(1)} all-reduce(f32[1,3,2,768]{3,2,1,0:T(2,128)S(1)} %all_gather_reshape.3), channel_id=1, replica_groups=mesh['rep'=2,'fs'=8,'tp'=2] {'fs'}, use_global_device_ids=true, to_apply=%region_5.6 | all-reduce | flops 4608 | bytes 36864 | tf_op jit(solution)/shard_map/psum | solution.py:117
  243.7 4.4 %all_gather.17 = f32[2,3,2,768]{3,2,1,0:T(2,128)S(1)} all-gather(f32[1,3,2,768]{3,2,1,0:T(2,128)S(1)} %psum.7), channel_id=1, replica_groups=mesh['rep'=2,'fs'=8,'tp'=2] {'rep'}, dimensions={0}, use_global_device_ids=true | all-gather | bytes 55296 | tf_op jit(solution)/shard_map/all_gather | solution.py:118
  248.1 1.8 all-gather
  250.0 1.2 slice.184
  252.1 79.1 %reduce-scatter.5.cloned.1.call-done = bf16[256,1536]{1,0:T(8,128)(2,1)} async-done(((bf16[2048,1536]{1,0:T(8,128)(2,1)}), bf16[256,1536]{1,0:T(8,128)(2,1)}) %reduce-scatter.5.cloned.1.call-update) | async-done | bytes 786448 | tf_op jit(solution)/shard_map/reduce_scatter | solution.py:92
  332.4 2.3 fusion.20
  336.0 3.1 dynamic_update_slice.12
  339.2 3.1 dynamic_update_slice.14
  342.3 7.6 %collective-permute-done.7 = bf16[256,1536]{1,0:T(8,128)(2,1)S(1)} collective-permute-done((bf16[256,1536]{1,0:T(8,128)(2,1)}, bf16[256,1536]{1,0:T(8,128)(2,1)S(1)}, u32[]{:S(2)}, u32[]{:S(2)}) %collective-permute-start.7) | collective-permute-done | bytes 786464 | tf_op jit(solution)/shard_map/ppermute | solution.py:11
  350.4 4.4 %dynamic_update_slice.13 = bf16[256,1408]{1,0:T(8,128)(2,1)S(1)} dynamic-update-slice(bf16[256,1408]{1,0:T(8,128)(2,1)S(1)} %dynamic_update_slice.12, bf16[256,768]{1,0:T(8,128)(2,1)S(1)} %get-tuple-element.27, s32[]{:T(128)} %constant.42.clone.1, s32[]{:T(128)S(6)} %select_n.71) | dynamic-update-slice | bytes 786436 | tf_op jit(solution)/shard_map/dynamic_update_slice | solution.py:115
  356.0 4.3 %dynamic_update_slice.15 = bf16[256,1408]{1,0:T(8,128)(2,1)S(1)} dynamic-update-slice(bf16[256,1408]{1,0:T(8,128)(2,1)S(1)} %dynamic_update_slice.14, bf16[256,768]{1,0:T(8,128)(2,1)S(1)} %get-tuple-element.26, s32[]{:T(128)} %constant.42.clone.1, s32[]{:T(128)S(6)} %select_n.71) | dynamic-update-slice | bytes 786436 | tf_op jit(solution)/shard_map/dynamic_update_slice | solution.py:115
  (57 shorter events, 13.4 us)
Async XLA Ops:
  7.2 56.6 %all-gather.4.cloned.1.call-start = ((), (), s32[]{:S(2)}) async-start(), calls=%async_computation.2 | async-start | bytes 6291456 | tf_op jit(solution)/shard_map/all_gather | solution.py:63
  8.8 14.6 %collective-permute-start.4 = (bf16[8,1024]{0,1:T(8,128)(2,1)S(1)}, bf16[8,1024]{0,1:T(8,128)(2,1)S(1)}, u32[]{:S(2)}, u32[]{:S(2)}) collective-permute-start(bf16[8,1024]{0,1:T(8,128)(2,1)S(1)} %get-tuple-element.31), channel_id=1, source_target_pairs={{0,2},{2,4},{4,6},{6,8},{8,10},{10,12},{12,14},{1,3},{3,5},{5,7},{... | collective-permute-start | bytes 49160 | tf_op jit(solution)/shard_map/ppermute | solution.py:17
  12.3 11.2 %collective-permute-start.3 = (bf16[8,1024]{0,1:T(8,128)(2,1)S(1)}, bf16[8,1024]{0,1:T(8,128)(2,1)S(1)}, u32[]{:S(2)}, u32[]{:S(2)}) collective-permute-start(bf16[8,1024]{0,1:T(8,128)(2,1)S(1)} %get-tuple-element.30), channel_id=1, source_target_pairs={{2,0},{4,2},{6,4},{8,6},{10,8},{12,10},{14,12},{3,1},{5,3},{7,5},{... | collective-permute-start | bytes 49160 | tf_op jit(solution)/shard_map/ppermute | solution.py:16
  24.1 17.5 %collective-permute-start.5 = (bf16[400,1024]{1,0:T(8,128)(2,1)S(1)}, bf16[400,1024]{1,0:T(8,128)(2,1)}, u32[]{:S(2)}, u32[]{:S(2)}) collective-permute-start(bf16[400,1024]{1,0:T(8,128)(2,1)S(1)} %copy.21), channel_id=1, source_target_pairs={{0,16},{16,0},{1,17},{17,1},{2,18},{18,2},{3,19},{19,3},{4,20},{20... | collective-permute-start | bytes 2457608 | tf_op jit(solution)/shard_map/ppermute | solution.py:11
  43.1 4.2 %copy-start.1 = (bf16[1,384,1408]{2,1,0:T(8,128)(2,1)S(1)}, bf16[1,384,1408]{2,1,0:T(8,128)(2,1)}, u32[]{:S(2)}) copy-start(bf16[1,384,1408]{2,1,0:T(8,128)(2,1)} %param.11) | copy-start | bytes 3244036
  44.7 121.4 %all-gather.6.cloned.1.call-start = ((), (), s32[]{:S(2)}) async-start(), calls=%async_computation.3 | async-start | bytes 7077888 | tf_op jit(solution)/shard_map/all_gather | solution.py:56
  47.2 202.8 %reduce-scatter.3.cloned.1.call-start = ((), (), s32[]{:S(2)}) async-start(), calls=%async_computation.4 | async-start | bytes 4718592 | tf_op jit(solution)/shard_map/reduce_scatter | solution.py:96
  47.3 8.5 %collective-permute-start.1 = (bf16[8,1408]{1,0:T(8,128)(2,1)S(1)}, bf16[8,1408]{1,0:T(8,128)(2,1)S(1)}, u32[]{:S(2)}, u32[]{:S(2)}) collective-permute-start(bf16[8,1408]{1,0:T(8,128)(2,1)S(1)} %get-tuple-element.25), channel_id=1, source_target_pairs={{0,2},{2,4},{4,6},{6,8},{8,10},{10,12},{12,14},{1,3},{3,5},{5,7},{... | collective-permute-start | bytes 67592 | tf_op jit(solution)/shard_map/ppermute | solution.py:17
  53.5 7.1 %collective-permute-start = (bf16[8,1408]{1,0:T(8,128)(2,1)S(1)}, bf16[8,1408]{1,0:T(8,128)(2,1)S(1)}, u32[]{:S(2)}, u32[]{:S(2)}) collective-permute-start(bf16[8,1408]{1,0:T(8,128)(2,1)S(1)} %get-tuple-element.24), channel_id=1, source_target_pairs={{2,0},{4,2},{6,4},{8,6},{10,8},{12,10},{14,12},{3,1},{5,3},{7,5},{... | collective-permute-start | bytes 67592 | tf_op jit(solution)/shard_map/ppermute | solution.py:16
  62.3 115.7 %collective-permute-start.2 = (bf16[400,768]{1,0:T(8,128)(2,1)}, bf16[400,768]{1,0:T(8,128)(2,1)}, u32[]{:S(2)}, u32[]{:S(2)}) collective-permute-start(bf16[400,768]{1,0:T(8,128)(2,1)} %get-tuple-element.23), channel_id=1, source_target_pairs={{0,16},{16,0},{1,17},{17,1},{2,18},{18,2},{3,19},{19,3},{4,20},{20... | collective-permute-start | bytes 1843208 | tf_op jit(solution)/shard_map/ppermute | solution.py:11
  176.3 1.7 copy-start
  198.9 132.3 %reduce-scatter.5.cloned.1.call-start = ((), (), s32[]{:S(2)}) async-start(), calls=%async_computation.5 | async-start | bytes 7077888 | tf_op jit(solution)/shard_map/reduce_scatter | solution.py:92
  251.3 81.2 %collective-permute-start.6 = (bf16[384,1024]{1,0:T(8,128)(2,1)S(1)}, bf16[384,1024]{1,0:T(8,128)(2,1)S(1)}, u32[]{:S(2)}, u32[]{:S(2)}) collective-permute-start(bf16[384,1024]{1,0:T(8,128)(2,1)S(1)} %slice.184), channel_id=1, source_target_pairs={{0,16},{16,0},{1,17},{17,1},{2,18},{18,2},{3,19},{19,3},{4,20},{20... | collective-permute-start | bytes 2359304 | tf_op jit(solution)/shard_map/ppermute | solution.py:11
  331.2 18.7 %collective-permute-start.7 = (bf16[256,1536]{1,0:T(8,128)(2,1)}, bf16[256,1536]{1,0:T(8,128)(2,1)S(1)}, u32[]{:S(2)}, u32[]{:S(2)}) collective-permute-start(bf16[256,1536]{1,0:T(8,128)(2,1)} %reduce-scatter.5.cloned.1.call-done), channel_id=1, source_target_pairs={{0,16},{16,0},{1,17},{17,1},{2,18},{18,2},{3,19},{19,3},{4,20},{20... | collective-permute-start | bytes 2359304 | tf_op jit(solution)/shard_map/ppermute | solution.py:11
Sparse Core Ops, SparseCore 0:
  44.8 18.8 all-gather.3
  66.5 99.5 all-gather.5
  199.0 9.4 reduce-scatter.2
  212.0 119.1 reduce-scatter.4
where the time goes:
time: 369 us; the launch traced here: 368 us
  waiting for transfers between devices  217 us (59%)
  blocking collectives  41.6 us (11%)
  local copies, waits for them, and re-layouts  29 us (8%)
  matrix products  26.4 us (7%)
  other arithmetic  24.7 us (7%)
  starting transfers between devices  15.3 us (4%)
  between operations  14.2 us (4%)
    all_gather x1, waiting for transfers between devices, shards(): w_all = lax.all_gather(w_own, 'fs', axis=0, tiled=True)  97.7 us
    reduce_scatter x1, waiting for transfers between devices, shards(): own = lax.psum_scatter(grads, 'fs', scatter_dimension=0, tiled=True)  79.1 us
    psum x1, blocking collectives, shards(): tap_sum = lax.psum(tap_terms * factor, 'fs').reshape(3, 2, width)  35.4 us
    ppermute x4, waiting for transfers between devices, shift(): lax.ppermute(x, axis, [(i, (i + step) % count) for i in range(count)])  24.4 us
    dynamic_update_slice x4, local copies, waits for them, and re-layouts, shards(): cols = lax.dynamic_update_slice_in_dim(cols, new, place, 1)  15 us
    ppermute x2, waiting for transfers between devices, with_halo(): lax.ppermute(rows[rows.shape[0] - HALO:], 'fs', [(i, i + 1) for i in rang...  9.85 us
    ppermute x2, starting transfers between devices, with_halo(): lax.ppermute(rows[rows.shape[0] - HALO:], 'fs', [(i, i + 1) for i in rang...  9.6 us
    dot_general x1, matrix products, shards(): lax.dot_general(pre_cot, w_all, contract_cols, preferred_element_type=jnp...  9.31 us
  transfers between devices with their start and end apart: 12, of which 7 were waited for; matrix products, arithmetic and copies ran while one was open for 12% of the time, Pallas kernels for 0%

commit v1 on v0

--- a/solution.py
+++ b/solution.py
@@ -53,7 +53,9 @@
         ],
         axis=1,
     )
-    w_all = lax.all_gather(w_own, "fs", axis=0, tiled=True)
+    w_all = jnp.concatenate(
+        lax.all_to_all(jnp.stack([w_own] * lax.axis_size("fs")), "fs", 0, 0), axis=0
+    )
     x_ext = with_halo(inputs[0])
     g_ext = with_halo(out_grad[0])
     x_blocks, g_blocks = ([x_ext], [part_cols(g_ext, rep)])

time: 369 us -> 409 us (1.11)
  starting transfers between devices: 15.3 us -> 69.6 us
  waiting for transfers between devices: 217 us -> 197 us
    all_gather x1 -> x0, waiting for transfers between devices: 97.7 us -> none  [shards(): w_all = lax.all_gather(w_own, 'fs', axis=0, tiled=True)]
    ppermute x2, starting transfers between devices: 9.6 us -> 58 us  [with_halo(): lax.ppermute(rows[rows.shape[0] - HALO:], 'fs', [(i, i + 1) for i in rang...]
    ppermute x2, waiting for transfers between devices: 9.85 us -> 52.8 us  [with_halo(): lax.ppermute(rows[rows.shape[0] - HALO:], 'fs', [(i, i + 1) for i in rang...]
    all_gather x1, waiting for transfers between devices: 0.86 us -> 34.2 us  [shards(): x_all = lax.all_gather(jnp.stack(x_blocks), 'tp', axis=2, tiled=True)]
    all_to_all x0 -> x1, starting transfers between devices: none -> 5.97 us  [shards(): lax.all_to_all(jnp.stack([w_own] * lax.axis_size('fs')), 'fs', 0, 0)]
  transfers between devices with their start and end apart: 12 -> 12, of which waited for: 7 -> 6; matrix products, arithmetic and copies ran while one was open for 12% -> 11% of each run, Pallas kernels for 0% -> 0%
where the time goes in v1:
time: 409 us; the launch traced here: 408 us
  waiting for transfers between devices  197 us (48%)
  starting transfers between devices  69.6 us (17%)
  blocking collectives  44.4 us (11%)
  local copies, waits for them, and re-layouts  31.8 us (8%)
  matrix products  26.5 us (6%)
  other arithmetic  24.8 us (6%)
  between operations  14.2 us (3%)
    reduce_scatter x1, waiting for transfers between devices, shards(): own = lax.psum_scatter(grads, 'fs', scatter_dimension=0, tiled=True)  79.3 us
    ppermute x2, starting transfers between devices, with_halo(): lax.ppermute(rows[rows.shape[0] - HALO:], 'fs', [(i, i + 1) for i in rang...  58 us
    ppermute x2, waiting for transfers between devices, with_halo(): lax.ppermute(rows[rows.shape[0] - HALO:], 'fs', [(i, i + 1) for i in rang...  52.8 us
    psum x1, blocking collectives, shards(): tap_sum = lax.psum(tap_terms * factor, 'fs').reshape(3, 2, width)  38.2 us
    all_gather x1, waiting for transfers between devices, shards(): x_all = lax.all_gather(jnp.stack(x_blocks), 'tp', axis=2, tiled=True)  34.2 us
    ppermute x4, waiting for transfers between devices, shift(): lax.ppermute(x, axis, [(i, (i + step) % count) for i in range(count)])  25.4 us
    dynamic_update_slice x4, local copies, waits for them, and re-layouts, shards(): cols = lax.dynamic_update_slice_in_dim(cols, new, place, 1)  15 us
    dot_general x1, matrix products, shards(): lax.dot_general(pre_cot, w_all, contract_cols, preferred_element_type=jnp...  9.33 us
  transfers between devices with their start and end apart: 12, of which 6 were waited for; matrix products, arithmetic and copies ran while one was open for 11% of the time, Pallas kernels for 0%

profile of v1, /device:TPU:2, one launch (start us, length us, event | category | flops | bytes accessed | tf_op | source)
XLA Modules:
  0.0 408.5 jit_solution(7205016108748961164)
XLA Ops:
  7.2 1.5 dynamic-slice_select_fusion.1
  8.8 3.2 stack.47
  11.9 6.0 %all-to-all-start = ((bf16[8,256,1536]{2,1,0:T(8,128)(2,1)}), bf16[8,256,1536]{2,1,0:T(8,128)(2,1)}, u32[]{:S(2)}, u32[]{:S(2)}) async-start(bf16[8,256,1536]{2,1,0:T(8,128)(2,1)} %stack.47), calls=%async_computation | async-start | bytes 12582912 | tf_op jit(solution)/shard_map/all_to_all | solution.py:57
  18.4 3.9 collective-permute-start.4
  22.4 1.3 collective-permute-start.3
  23.7 52.8 %collective-permute-done.4 = bf16[8,1024]{0,1:T(8,128)(2,1)S(1)} collective-permute-done((bf16[8,1024]{0,1:T(8,128)(2,1)S(1)}, bf16[8,1024]{0,1:T(8,128)(2,1)S(1)}, u32[]{:S(2)}, u32[]{:S(2)}) %collective-permute-start.4) | collective-permute-done | bytes 16416 | tf_op jit(solution)/shard_map/ppermute | solution.py:17
  79.6 17.7 %collective-permute-done.5 = bf16[400,1024]{1,0:T(8,128)(2,1)} collective-permute-done((bf16[400,1024]{1,0:T(8,128)(2,1)}, bf16[400,1024]{1,0:T(8,128)(2,1)}, u32[]{:S(2)}, u32[]{:S(2)}) %collective-permute-start.5) | collective-permute-done | bytes 819232 | tf_op jit(solution)/shard_map/ppermute | solution.py:11
  97.4 1.4 copy.22
  98.8 1.6 pad_maximum_fusion.4
  100.5 54.1 %collective-permute-start.1 = (bf16[8,1408]{1,0:T(8,128)(2,1)S(1)}, bf16[8,1408]{1,0:T(8,128)(2,1)S(1)}, u32[]{:S(2)}, u32[]{:S(2)}) collective-permute-start(bf16[8,1408]{1,0:T(8,128)(2,1)S(1)} %get-tuple-element.25), channel_id=1, source_target_pairs={{0,2},{2,4},{4,6},{6,8},{8,10},{10,12},{12,14},{1,3},{3,5},{5,7},{... | collective-permute-start | bytes 67592 | tf_op jit(solution)/shard_map/ppermute | solution.py:17
  154.6 1.5 collective-permute-start
  156.9 5.4 %collective-permute-done = bf16[8,1408]{1,0:T(8,128)(2,1)S(1)} collective-permute-done((bf16[8,1408]{1,0:T(8,128)(2,1)S(1)}, bf16[8,1408]{1,0:T(8,128)(2,1)S(1)}, u32[]{:S(2)}, u32[]{:S(2)}) %collective-permute-start) | collective-permute-done | bytes 22560 | tf_op jit(solution)/shard_map/ppermute | solution.py:16
  162.4 1.6 dynamic-slice_bitcast_fusion
  164.6 34.2 %all-gather.3.cloned.1.call-done = bf16[2,400,2048]{1,2,0:T(8,128)(2,1)} async-done(((bf16[2,400,1024]{1,2,0:T(8,128)(2,1)}), bf16[2,400,2048]{1,2,0:T(8,128)(2,1)}) %all-gather.3.cloned.1.call-update) | async-done | bytes 3276816 | tf_op jit(solution)/shard_map/all_gather | solution.py:65
  198.8 4.7 %copy.23 = bf16[2,400,2048]{2,1,0:T(8,128)(2,1)S(1)} copy(bf16[2,400,2048]{1,2,0:T(8,128)(2,1)} %all-gather.3.cloned.1.call-done) | data formatting | bytes 6553600 | tf_op jit(solution)/shard_map/all_gather | solution.py:65
  203.5 8.2 %convolution_convert_fusion = bf16[800,1536]{1,0:T(8,128)(2,1)S(1)} fusion(bf16[800,2048]{1,0:T(8,128)(2,1)S(1)} %bitcast.56, bf16[2048,1536]{1,0:T(8,128)(2,1)} %bitcast.11), kind=kOutput, calls=%fused_computation.37 | convolution fusion | flops 5034393600 | bytes 12025856 | tf_op jit(solution)/shard_map/dot_general | solution.py:68
  212.4 1.3 fusion.24
  213.7 1.7 fusion.3
  215.4 2.2 convert_multiply_fusion
  218.8 8.2 %fusion.15 = (f32[1536]{0:T(1024)S(1)}, f32[1536]{0:T(1024)S(1)}, f32[1536]{0:T(1024)S(1)}, bf16[2,384,1536]{2,1,0:T(8,128)(2,1)S(1)}) fusion(f32[2,400,1536]{2,1,0:T(8,128)S(1)} %convert.5, f32[2,400,768]{2,1,0:T(8,128)S(1)} %get-tuple-element.11, f32[2,400,768]{2,1,0:T(8,128)S(1)} %get-tuple-element.12, f32[2,399,1536]{2,1,0:T(8,128)S(1)} %get-tuple-element.18, ...), kind=kLoop, calls=%fused_computation.31 | loop fusion | flops 20049408 | bytes 31494144 | tf_op jit(solution)/shard_map/reduce_sum | solution.py:84
  227.0 9.3 %convolution_convert_fusion.1 = bf16[768,2048]{1,0:T(8,128)(2,1)} fusion(bf16[768,1536]{1,0:T(8,128)(2,1)S(1)} %bitcast.57, bf16[2048,1536]{1,0:T(8,128)(2,1)} %bitcast.11), kind=kOutput, calls=%fused_computation.38 | convolution fusion | flops 4833411072 | bytes 11796480 | tf_op jit(solution)/shard_map/dot_general | solution.py:95
  236.6 9.0 %fusion = bf16[2048,1536]{1,0:T(8,128)(2,1)} fusion(bf16[2,384,1536]{2,1,0:T(8,128)(2,1)S(1)} %get-tuple-element.13, bf16[2,400,2048]{1,2,0:T(8,128)(2,1)} %all-gather.3.cloned.1.call-done), kind=kOutput, calls=%fused_computation.1 | convolution fusion | flops 4838129664 | bytes 11796480 | tf_op jit(solution)/shard_map/dot_general | solution.py:87
  245.8 38.2 %psum.7 = f32[1,3,2,768]{3,2,1,0:T(2,128)S(1)} all-reduce(f32[1,3,2,768]{3,2,1,0:T(2,128)S(1)} %all_gather_reshape.3), channel_id=1, replica_groups=mesh['rep'=2,'fs'=8,'tp'=2] {'fs'}, use_global_device_ids=true, to_apply=%region_5.6 | all-reduce | flops 4608 | bytes 36864 | tf_op jit(solution)/shard_map/psum | solution.py:119
  283.9 4.4 %all_gather.13 = f32[2,3,2,768]{3,2,1,0:T(2,128)S(1)} all-gather(f32[1,3,2,768]{3,2,1,0:T(2,128)S(1)} %psum.7), channel_id=1, replica_groups=mesh['rep'=2,'fs'=8,'tp'=2] {'rep'}, dimensions={0}, use_global_device_ids=true | all-gather | bytes 55296 | tf_op jit(solution)/shard_map/all_gather | solution.py:120
  288.4 1.8 all-gather
  292.4 79.3 %reduce-scatter.5.cloned.1.call-done = bf16[256,1536]{1,0:T(8,128)(2,1)} async-done(((bf16[2048,1536]{1,0:T(8,128)(2,1)}), bf16[256,1536]{1,0:T(8,128)(2,1)}) %reduce-scatter.5.cloned.1.call-update) | async-done | bytes 786448 | tf_op jit(solution)/shard_map/reduce_scatter | solution.py:94
  372.9 2.3 fusion.20
  376.4 3.1 dynamic_update_slice.12
  379.6 3.1 dynamic_update_slice.14
  382.7 7.6 %collective-permute-done.7 = bf16[256,1536]{1,0:T(8,128)(2,1)S(1)} collective-permute-done((bf16[256,1536]{1,0:T(8,128)(2,1)}, bf16[256,1536]{1,0:T(8,128)(2,1)S(1)}, u32[]{:S(2)}, u32[]{:S(2)}) %collective-permute-start.7) | collective-permute-done | bytes 786464 | tf_op jit(solution)/shard_map/ppermute | solution.py:11
  390.8 4.4 %dynamic_update_slice.13 = bf16[256,1408]{1,0:T(8,128)(2,1)S(1)} dynamic-update-slice(bf16[256,1408]{1,0:T(8,128)(2,1)S(1)} %dynamic_update_slice.12, bf16[256,768]{1,0:T(8,128)(2,1)S(1)} %get-tuple-element.27, s32[]{:T(128)} %constant.42.clone.1, s32[]{:T(128)S(6)} %select_n.71) | dynamic-update-slice | bytes 786436 | tf_op jit(solution)/shard_map/dynamic_update_slice | solution.py:117
  396.4 4.3 %dynamic_update_slice.15 = bf16[256,1408]{1,0:T(8,128)(2,1)S(1)} dynamic-update-slice(bf16[256,1408]{1,0:T(8,128)(2,1)S(1)} %dynamic_update_slice.14, bf16[256,768]{1,0:T(8,128)(2,1)S(1)} %get-tuple-element.26, s32[]{:T(128)} %constant.42.clone.1, s32[]{:T(128)S(6)} %select_n.71) | dynamic-update-slice | bytes 786436 | tf_op jit(solution)/shard_map/dynamic_update_slice | solution.py:117
  (61 shorter events, 14.9 us)
Async XLA Ops:
  11.9 6.0 %copy-start.3 = (bf16[1,384,1024]{2,1,0:T(8,128)(2,1)S(1)}, bf16[1,384,1024]{2,1,0:T(8,128)(2,1)}, u32[]{:S(2)}) copy-start(bf16[1,384,1024]{2,1,0:T(8,128)(2,1)} %param.6) | copy-start | bytes 2359300
  11.9 191.6 %all-to-all-start = ((bf16[8,256,1536]{2,1,0:T(8,128)(2,1)}), bf16[8,256,1536]{2,1,0:T(8,128)(2,1)}, u32[]{:S(2)}, u32[]{:S(2)}) async-start(bf16[8,256,1536]{2,1,0:T(8,128)(2,1)} %stack.47), calls=%async_computation | async-start | bytes 12582912 | tf_op jit(solution)/shard_map/all_to_all | solution.py:57
  17.9 180.9 %all-gather.3.cloned.1.call-start = ((), (), s32[]{:S(2)}) async-start(), calls=%async_computation.3 | async-start | bytes 6291456 | tf_op jit(solution)/shard_map/all_gather | solution.py:65
  18.4 58.0 %collective-permute-start.4 = (bf16[8,1024]{0,1:T(8,128)(2,1)S(1)}, bf16[8,1024]{0,1:T(8,128)(2,1)S(1)}, u32[]{:S(2)}, u32[]{:S(2)}) collective-permute-start(bf16[8,1024]{0,1:T(8,128)(2,1)S(1)} %get-tuple-element.31), channel_id=1, source_target_pairs={{0,2},{2,4},{4,6},{6,8},{8,10},{10,12},{12,14},{1,3},{3,5},{5,7},{... | collective-permute-start | bytes 49160 | tf_op jit(solution)/shard_map/ppermute | solution.py:17
  22.4 54.1 %collective-permute-start.3 = (bf16[8,1024]{0,1:T(8,128)(2,1)S(1)}, bf16[8,1024]{0,1:T(8,128)(2,1)S(1)}, u32[]{:S(2)}, u32[]{:S(2)}) collective-permute-start(bf16[8,1024]{0,1:T(8,128)(2,1)S(1)} %get-tuple-element.30), channel_id=1, source_target_pairs={{2,0},{4,2},{6,4},{8,6},{10,8},{12,10},{14,12},{3,1},{5,3},{7,5},{... | collective-permute-start | bytes 49160 | tf_op jit(solution)/shard_map/ppermute | solution.py:16
  76.5 1.4 copy-start.2
  77.9 22.5 %copy-start.1 = (bf16[1,384,1408]{2,1,0:T(8,128)(2,1)S(1)}, bf16[1,384,1408]{2,1,0:T(8,128)(2,1)}, u32[]{:S(2)}) copy-start(bf16[1,384,1408]{2,1,0:T(8,128)(2,1)} %param.11) | copy-start | bytes 3244036
  77.9 19.4 %collective-permute-start.5 = (bf16[400,1024]{1,0:T(8,128)(2,1)}, bf16[400,1024]{1,0:T(8,128)(2,1)}, u32[]{:S(2)}, u32[]{:S(2)}) collective-permute-start(bf16[400,1024]{1,0:T(8,128)(2,1)} %copy.21), channel_id=1, source_target_pairs={{0,16},{16,0},{1,17},{17,1},{2,18},{18,2},{3,19},{19,3},{4,20},{20... | collective-permute-start | bytes 2457608 | tf_op jit(solution)/shard_map/ppermute | solution.py:11
  100.4 189.9 %reduce-scatter.3.cloned.1.call-start = ((), (), s32[]{:S(2)}) async-start(), calls=%async_computation.4 | async-start | bytes 4718592 | tf_op jit(solution)/shard_map/reduce_scatter | solution.py:98
  100.5 56.5 %collective-permute-start.1 = (bf16[8,1408]{1,0:T(8,128)(2,1)S(1)}, bf16[8,1408]{1,0:T(8,128)(2,1)S(1)}, u32[]{:S(2)}, u32[]{:S(2)}) collective-permute-start(bf16[8,1408]{1,0:T(8,128)(2,1)S(1)} %get-tuple-element.25), channel_id=1, source_target_pairs={{0,2},{2,4},{4,6},{6,8},{8,10},{10,12},{12,14},{1,3},{3,5},{5,7},{... | collective-permute-start | bytes 67592 | tf_op jit(solution)/shard_map/ppermute | solution.py:17
  154.6 7.8 %collective-permute-start = (bf16[8,1408]{1,0:T(8,128)(2,1)S(1)}, bf16[8,1408]{1,0:T(8,128)(2,1)S(1)}, u32[]{:S(2)}, u32[]{:S(2)}) collective-permute-start(bf16[8,1408]{1,0:T(8,128)(2,1)S(1)} %get-tuple-element.24), channel_id=1, source_target_pairs={{2,0},{4,2},{6,4},{8,6},{10,8},{12,10},{14,12},{3,1},{5,3},{7,5},{... | collective-permute-start | bytes 67592 | tf_op jit(solution)/shard_map/ppermute | solution.py:16
  164.0 51.4 %collective-permute-start.2 = (bf16[400,768]{1,0:T(8,128)(2,1)}, bf16[400,768]{1,0:T(8,128)(2,1)}, u32[]{:S(2)}, u32[]{:S(2)}) collective-permute-start(bf16[400,768]{1,0:T(8,128)(2,1)} %get-tuple-element.23), channel_id=1, source_target_pairs={{0,16},{16,0},{1,17},{17,1},{2,18},{18,2},{3,19},{19,3},{4,20},{20... | collective-permute-start | bytes 1843208 | tf_op jit(solution)/shard_map/ppermute | solution.py:11
  213.7 1.7 copy-start
  236.3 135.3 %reduce-scatter.5.cloned.1.call-start = ((), (), s32[]{:S(2)}) async-start(), calls=%async_computation.5 | async-start | bytes 7077888 | tf_op jit(solution)/shard_map/reduce_scatter | solution.py:94
  291.5 81.3 %collective-permute-start.6 = (bf16[384,1024]{1,0:T(8,128)(2,1)S(1)}, bf16[384,1024]{1,0:T(8,128)(2,1)S(1)}, u32[]{:S(2)}, u32[]{:S(2)}) collective-permute-start(bf16[384,1024]{1,0:T(8,128)(2,1)S(1)} %slice.184), channel_id=1, source_target_pairs={{0,16},{16,0},{1,17},{17,1},{2,18},{18,2},{3,19},{19,3},{4,20},{20... | collective-permute-start | bytes 2359304 | tf_op jit(solution)/shard_map/ppermute | solution.py:11
  371.6 18.7 %collective-permute-start.7 = (bf16[256,1536]{1,0:T(8,128)(2,1)}, bf16[256,1536]{1,0:T(8,128)(2,1)S(1)}, u32[]{:S(2)}, u32[]{:S(2)}) collective-permute-start(bf16[256,1536]{1,0:T(8,128)(2,1)} %reduce-scatter.5.cloned.1.call-done), channel_id=1, source_target_pairs={{0,16},{16,0},{1,17},{17,1},{2,18},{18,2},{3,19},{19,3},{4,20},{20... | collective-permute-start | bytes 2359304 | tf_op jit(solution)/shard_map/ppermute | solution.py:11
Sparse Core Ops, SparseCore 0:
  100.5 98.2 all-gather.2
  236.5 12.2 reduce-scatter.2
  252.3 119.2 reduce-scatter.4
